TPU v7x, 512 devices: a whole 4x4x16 slice. The times are simulated.
512 devices in a mesh: sp: 32 (over z, core), tp: 16 (over y, x).
Axes of the slice: x: 4, y: 4, z: 16, core: 2. Of those that a mesh axis runs over, the one named last changes fastest.
Arguments:
- residual: bfloat16 [6144, 2048], P('sp'), may hold values from -6 to 6
- query_in: bfloat16 [6144, 2048], P('sp', 'tp'), may hold values from -6 to 6
- value_in: bfloat16 [6144, 2048], P('sp', 'tp'), may hold values from -6 to 6
- forget_fwd: bfloat16 [6144, 2048], P('sp', 'tp'), may hold values from -4.5 to 4.5
- forget_bwd: bfloat16 [6144, 2048], P('sp', 'tp'), may hold values from -4.5 to 4.5
- jumps: float32 [16, 6144], P('tp', 'sp'), may hold values from -2.8 to 0
- gate_gap: float32 [2, 2048], P(None, 'tp'), may hold values from 0 to 0.1
- out_gate: bfloat16 [6144, 2048], P('sp', 'tp'), may hold values from -6 to 6
- head_gain: float32 [2048], P('tp'), may hold values from 0.1 to 1.9
- out_weight: bfloat16 [2048, 2048], P('tp'), may hold values from -0.25 to 0.25
- norm_gain: float32 [2048], replicated, may hold values from 0.1 to 1.9
- route_ids: int32 [6144, 4], P('sp'), may hold values from 0 to 31, all different within a row; in each aligned block of 192 rows (0 to 191, 192 to 383, ...) at most 36 rows name the same one
- route_weights: float32 [6144, 4], P('sp'), may hold values from 0.05 to 0.5
- w_gate: bfloat16 [32, 2048, 4096], P('sp', None, 'tp'), may hold values from -0.375 to 0.375
- w_up: bfloat16 [32, 2048, 4096], P('sp', None, 'tp'), may hold values from -0.375 to 0.375
- w_down: bfloat16 [32, 4096, 2048], P('sp', None, 'tp'), may hold values from -0.09375 to 0.09375
Outputs:
- mixed: bfloat16 [6144, 2048], P('sp', 'tp')
Inputs may be any that keep to these rules, and one draw needn't show every extreme that they name: `route_ids`: in each aligned block of 192 rows each expert is named by at most 36 rows, and by exactly 36 in some block; each row names 4 different experts.
All inputs are finite; a program needn't handle non-finite values.
Results may differ from a plain program's by a relative error of at most 0.024.
Values may be sent and summed in bfloat16 or wider, within the bound.
A program may use at most 64 MiB of HBM per device.

v0:
```python
import math
import jax
import jax.numpy as jnp
from jax import lax
from jax.sharding import Mesh
from jax.sharding import PartitionSpec as P

EXPERTS = 32
CAP = 36
SP = ("sp_0", "sp_1")
highest_precision = lax.Precision.HIGHEST
eps_norm = 1e-06
limit_value = 7.0
alpha_value = 1.702


def filled_with(x, identity):
    return jax.tree.map(
        lambda a, e: jnp.broadcast_to(jnp.asarray(e, a.dtype), a.shape), x, identity
    )


def all_in_one(x, axis):
    leaves = jax.tree.leaves(x)
    turns = sorted(range(len(leaves)), key=lambda k: -leaves[k].size)
    width = (1, *leaves[turns[0]].shape)[-1]
    lines = [
        jnp.pad(leaves[k].reshape(-1), (0, -leaves[k].size % width)).reshape(-1, width)
        for k in turns
    ]
    both, at, found = (lax.all_gather(jnp.concatenate(lines), axis), 0, {})
    for k, line in zip(turns, lines):
        section = both[:, at : at + len(line)].reshape(len(both), -1)
        found[k] = section[:, : leaves[k].size].reshape(-1, *leaves[k].shape)
        at += len(line)
    numbers = iter(range(len(leaves)))
    return jax.tree.map(lambda _: found[next(numbers)], x)


def entering(x, axes, combine, identity, reverse):
    before = start = filled_with(x, identity)
    running = x
    for axis in reversed(axes):
        length, index = (lax.axis_size(axis), lax.axis_index(axis))
        pieces = all_in_one(
            jax.tree.map(
                lambda part, kind: part.astype(kind),
                running,
                jax.tree.map(lambda a: jnp.bfloat16 if a.dtype == jnp.float32 else a.dtype, x),
            ),
            axis,
        )
        inside, running = (start, start)
        for k in reversed(range(length)) if reverse else range(length):
            passed = k > index if reverse else k < index
            running = combine(
                running, jax.tree.map(lambda part, own: part[k].astype(own.dtype), pieces, x)
            )
            inside = jax.tree.map(lambda new, old: jnp.where(passed, new, old), running, inside)
        before = combine(inside, before)
    return before


def in_blocks(x, dim, length):
    shape = x.shape
    pieces = x.reshape(*shape[:dim], length, shape[dim] // length, *shape[dim + 1 :])
    return jnp.moveaxis(pieces, dim, 0)


def sent_and_summed(x, axis, dim):
    length = lax.axis_size(axis)
    pieces = lax.all_to_all(in_blocks(x, dim, length), axis, 0, 0, tiled=True)
    return jnp.sum(pieces.astype(jnp.float32), axis=0)


def rows_for(lines, length):
    spare = -lines.shape[0] % length
    if not spare:
        return lines
    return jnp.concatenate([lines, jnp.zeros((spare, *lines.shape[1:]), lines.dtype)])


def in_order(pieces, dim):
    pieces = jnp.moveaxis(pieces, 0, dim)
    shape = pieces.shape
    return pieces.reshape(*shape[:dim], shape[dim] * shape[dim + 1], *shape[dim + 2 :])


def sent_to_all(x, axis):
    copies = jnp.broadcast_to(x, (lax.axis_size(axis), *x.shape))
    return lax.all_to_all(copies, axis, split_axis=0, concat_axis=0, tiled=True)


def gather_directly(x, axis, dim):
    return in_order(sent_to_all(x, axis), dim)


def sum_by_parts(x, axes):
    lines = x.reshape(-1, x.shape[-1])
    own = sent_and_summed(rows_for(lines, lax.axis_size(axes)), axes, 0)
    whole = gather_directly(own.astype(jnp.bfloat16), axes, 0)
    return whole[: len(lines)].reshape(x.shape).astype(jnp.float32)


def turned_blocks(pieces, axes, turns):
    inside = pieces.shape[1:]
    filled = pieces.reshape(*(lax.axis_size(a) for a in axes), *inside)
    for k in turns:
        filled = lax.all_to_all(filled, axes[k], k, k, tiled=True)
    return filled.reshape(-1, *inside)


def core_and_chips(x, groups, turns, split_dim, concat_dim):
    length = lax.axis_size(groups[0]) * lax.axis_size(groups[1])
    pieces = in_blocks(x, split_dim, length)
    return in_order(turned_blocks(pieces, groups, turns), concat_dim)


def block_pass(queries, keys_in, values, logs):
    head_rows, head_count, head_width = queries.shape
    block_size = math.gcd(head_rows, 64)
    block_count = head_rows // block_size

    def to_blocks(array):
        return array.reshape(block_count, block_size, head_count, array.shape[-1])

    q_block, k_block, v_block, log_block = (
        to_blocks(queries),
        to_blocks(keys_in),
        to_blocks(values),
        to_blocks(logs),
    )
    decay_sums = jnp.cumsum(log_block, axis=1)
    middle = decay_sums[:, block_size // 2 - 1 : block_size // 2]
    scores = jnp.einsum(
        "nthk,nshk->nhts",
        q_block * jnp.exp(decay_sums - middle),
        k_block * jnp.exp(middle - decay_sums),
        precision=highest_precision,
    )
    lower_mask = jnp.tril(jnp.ones((block_size, block_size), bool))
    within = jnp.einsum(
        "nhts,nshv->nthv", jnp.where(lower_mask, scores, 0.0), v_block, precision=highest_precision
    )
    block_end = decay_sums[:, -1]
    q_start = q_block * jnp.exp(decay_sums)
    k_end = k_block * jnp.exp(block_end[:, None] - decay_sums)

    def advance(current_state, block_items):
        query_segment, key_segment, value_segment, decay_part = block_items
        state_readout = jnp.einsum(
            "qwe,wei->qwi", query_segment, current_state, precision=highest_precision
        )
        current_state = current_state * jnp.exp(decay_part)[:, :, None] + jnp.einsum(
            "foj,fox->ojx", key_segment, value_segment, precision=highest_precision
        )
        return (current_state, state_readout)

    zero_state = jnp.zeros((head_count, head_width, values.shape[-1]), jnp.float32)
    final_state, across = lax.scan(advance, zero_state, (q_start, k_end, v_block, block_end))
    return ((within + across).reshape(head_rows, head_count, -1), final_state)


def combine_states(first_part, second_part):
    return (
        first_part[0] * second_part[0],
        second_part[0][:, :, None] * first_part[1] + second_part[1],
    )


def carried(queries, logs, running_state):
    decayed_state = queries * jnp.exp(jnp.cumsum(logs, axis=0))
    return jnp.einsum("una,nae->une", decayed_state, running_state, precision=highest_precision)


def shards(
    residual,
    query_in,
    value_in,
    forget_fwd,
    forget_bwd,
    jumps,
    gate_gap,
    out_gate,
    head_gain,
    out_weight,
    norm_gain,
    route_ids,
    route_weights,
    w_gate,
    w_up,
    w_down,
):
    head_rows, local_width = query_in.shape
    head_count = jumps.shape[0]
    head_width = local_width // head_count

    def by_head(array):
        return array.astype(jnp.float32).reshape(head_rows, head_count, head_width)

    queries = jax.nn.silu(by_head(query_in))
    values = by_head(value_in)
    jump_rows = jnp.transpose(jumps)[:, :, None]

    def gate_terms(forget_in, gap):
        key_share = gap.reshape(head_count, head_width) * jax.nn.sigmoid(-by_head(forget_in))
        return (key_share, jnp.log1p(-key_share) + jump_rows)

    keys_fwd, logs_fwd = gate_terms(forget_fwd, gate_gap[0])
    keys_bwd, logs_bwd = gate_terms(forget_bwd, gate_gap[1])
    ones_part = jnp.ones((head_count, head_width), jnp.float32)
    zero_part = jnp.zeros((head_count, head_width, head_width), jnp.float32)
    local_fwd, final_fwd = block_pass(queries, keys_fwd, values, logs_fwd)
    summary_fwd = (jnp.exp(jnp.sum(logs_fwd, axis=0)), final_fwd)
    carry_fwd = entering(summary_fwd, SP, combine_states, (ones_part, zero_part), False)[1]
    flip_queries = jnp.flip(queries, 0)
    flip_logs = jnp.flip(logs_bwd, 0)
    local_bwd, final_bwd = block_pass(
        flip_queries, jnp.flip(keys_bwd, 0), jnp.flip(values, 0), flip_logs
    )
    summary_bwd = (jnp.exp(jnp.sum(logs_bwd, axis=0)), final_bwd)
    carry_bwd = entering(summary_bwd, SP, combine_states, (ones_part, zero_part), True)[1]
    forward_out = local_fwd + carried(queries, logs_fwd, carry_fwd)
    backward_out = jnp.flip(local_bwd + carried(flip_queries, flip_logs, carry_bwd), 0)
    mixed_heads = forward_out + backward_out
    mean_square = jnp.mean(mixed_heads * mixed_heads, axis=-1, keepdims=True)
    normed = (mixed_heads * lax.rsqrt(mean_square + eps_norm)).reshape(head_rows, local_width)
    gated = (normed * head_gain * jax.nn.silu(out_gate.astype(jnp.float32))).astype(jnp.bfloat16)
    head_terms = jnp.dot(gated, out_weight, preferred_element_type=jnp.float32)
    summed = sum_by_parts(head_terms.astype(jnp.bfloat16), "tp")
    stream = (residual.astype(jnp.float32) + summed).astype(jnp.bfloat16)
    stream_f = stream.astype(jnp.float32)
    row_scale = lax.rsqrt(jnp.mean(stream_f * stream_f, axis=-1, keepdims=True) + eps_norm)
    normed_rows = (stream_f * row_scale * norm_gain).astype(jnp.bfloat16)
    top_count = route_ids.shape[1]
    flat_ids = route_ids.reshape(-1)
    one_hot = (flat_ids[:, None] == jnp.arange(EXPERTS, dtype=jnp.int32)[None, :]).astype(jnp.int32)
    slot_rank = jnp.sum((jnp.cumsum(one_hot, axis=0) - 1) * one_hot, axis=1)
    slot_index = flat_ids * CAP + slot_rank
    owner_rows = jnp.arange(head_rows * top_count, dtype=jnp.int32) // top_count
    slot_rows = jnp.full((EXPERTS * CAP,), head_rows, jnp.int32).at[slot_index].set(owner_rows)
    padded_rows = jnp.concatenate(
        [normed_rows, jnp.zeros((1, normed_rows.shape[1]), jnp.bfloat16)], axis=0
    )
    tp_index = lax.axis_index("tp")
    part_width = w_down.shape[2]
    column_rows = lax.dynamic_slice_in_dim(padded_rows, tp_index * part_width, part_width, 1)
    buffer = column_rows[slot_rows].reshape(EXPERTS, CAP, part_width)
    arrived = lax.all_to_all(buffer, SP, split_axis=0, concat_axis=1, tiled=True)
    piece = lax.all_gather(arrived, "tp", axis=2, tiled=True)
    gate_sum = jnp.einsum("esd,edf->esf", piece, w_gate, preferred_element_type=jnp.float32)
    up_sum = jnp.einsum("esd,edf->esf", piece, w_up, preferred_element_type=jnp.float32)
    gate_sum = jnp.minimum(gate_sum, limit_value)
    up_sum = jnp.clip(up_sum, -limit_value, limit_value)
    active = (gate_sum * jax.nn.sigmoid(alpha_value * gate_sum) * (up_sum + 1.0)).astype(
        jnp.bfloat16
    )
    produced = jnp.einsum(
        "esf,efd->esd",
        lax.all_gather(active, "tp", axis=2, tiled=True),
        w_down,
        preferred_element_type=jnp.float32,
    ).astype(jnp.bfloat16)
    returned = core_and_chips(produced, ("sp_0", "sp_1"), (1, 0), 1, 0)
    picked = returned.reshape(EXPERTS * CAP, part_width)[slot_index].astype(jnp.float32)
    picked = picked.reshape(head_rows, top_count, part_width)
    moe_out = jnp.sum(picked * route_weights[:, :, None], axis=1)
    own_columns = lax.dynamic_slice_in_dim(stream_f, tp_index * part_width, part_width, 1)
    return (own_columns + moe_out).astype(jnp.bfloat16)


def solution(mesh):
    finer = Mesh(mesh.devices.reshape(16, 2, mesh.shape["tp"]), ("sp_0", "sp_1", "tp"))
    return jax.shard_map(
        shards,
        mesh=finer,
        in_specs=(
            P(SP, None),
            P(SP, "tp"),
            P(SP, "tp"),
            P(SP, "tp"),
            P(SP, "tp"),
            P("tp", SP),
            P(None, "tp"),
            P(SP, "tp"),
            P("tp"),
            P("tp", None),
            P(),
            P(SP, None),
            P(SP, None),
            P(SP, None, "tp"),
            P(SP, None, "tp"),
            P(SP, None, "tp"),
        ),
        out_specs=P(SP, "tp"),
        check_vma=False,
    )
```

profile of v0, /device:TPU:2, one launch (start us, length us, event | category | flops | bytes accessed | tf_op | source)
XLA Modules:
  0.0 397.6 jit_solution(2136767596949991621)
XLA Ops:
  7.3 1.0 fusion.388
  10.9 1.7 while.26
  12.6 1.9 all-gather.5
  15.2 38.4 %all-gather.6 = bf16[16,129,128]{2,1,0:T(8,128)(2,1)S(1)} all-gather(bf16[1,129,128]{2,1,0:T(8,128)(2,1)S(1)} %maximum_bitcast_fusion.1), channel_id=3, replica_groups=mesh['sp_0'=16,'sp_1'=2,'tp'=16] {'sp_0'}, dimensions={0}, use_global_device_ids=true | all-gather | bytes 561408 | tf_op jit(solution)/shard_map/all_gather | solution.py:31
  56.6 1.7 while.27
  58.4 1.9 all-gather.7
  61.0 29.2 %all-gather.8 = bf16[16,129,128]{2,1,0:T(8,128)(2,1)S(1)} all-gather(bf16[1,129,128]{2,1,0:T(8,128)(2,1)S(1)} %maximum_bitcast_fusion.3), channel_id=5, replica_groups=mesh['sp_0'=16,'sp_1'=2,'tp'=16] {'sp_0'}, dimensions={0}, use_global_device_ids=true | all-gather | bytes 561408 | tf_op jit(solution)/shard_map/all_gather | solution.py:31
  92.2 1.1 fusion.41
  93.5 1.5 fusion.39
  96.0 1.6 multiply_reduce_fusion.1
  98.1 1.2 reshape.1657
  99.3 7.5 %all-to-all-start = ((bf16[16,12,2048]{2,1,0:T(8,128)(2,1)}), bf16[16,12,2048]{2,1,0:T(8,128)(2,1)S(1)}, u32[]{:S(2)}, u32[]{:S(2)}) async-start(bf16[16,12,2048]{2,1,0:T(8,128)(2,1)} %reshape.1657), calls=%async_computation | async-start | bytes 2097152 | tf_op jit(solution)/shard_map/all_to_all | solution.py:72
  107.0 1.7 reduce-window.26
  108.7 9.9 %all-to-all-done = bf16[16,12,2048]{2,1,0:T(8,128)(2,1)S(1)} async-done(((bf16[16,12,2048]{2,1,0:T(8,128)(2,1)}), bf16[16,12,2048]{2,1,0:T(8,128)(2,1)S(1)}, u32[]{:S(2)}, u32[]{:S(2)}) %all-to-all-start) | async-done | bytes 786464 | tf_op jit(solution)/shard_map/all_to_all | solution.py:72
  118.8 1.1 broadcast_in_dim.35
  120.0 5.0 %all-to-all-start.1 = ((bf16[16,12,2048]{2,1,0:T(8,128)(2,1)}), bf16[16,12,2048]{2,1,0:T(8,128)(2,1)S(1)}, u32[]{:S(2)}, u32[]{:S(2)}) async-start(bf16[16,12,2048]{2,1,0:T(8,128)(2,1)} %broadcast_in_dim.35), calls=%async_computation.1 | async-start | bytes 2097152 | tf_op jit(solution)/shard_map/all_to_all | solution.py:91
  125.7 3.4 scatter_custom_fusion
  129.2 7.8 %all-to-all-done.1 = bf16[16,12,2048]{2,1,0:T(8,128)(2,1)S(1)} async-done(((bf16[16,12,2048]{2,1,0:T(8,128)(2,1)}), bf16[16,12,2048]{2,1,0:T(8,128)(2,1)S(1)}, u32[]{:S(2)}, u32[]{:S(2)}) %all-to-all-start.1) | async-done | bytes 786464 | tf_op jit(solution)/shard_map/all_to_all | solution.py:91
  136.9 1.3 reshape.1699
  138.3 1.7 multiply_reduce_fusion
  140.2 2.9 gather_fusion
  143.2 33.2 %all_to_all.32 = bf16[32,36,128]{2,1,0:T(8,128)(2,1)S(1)} all-to-all(bf16[32,36,128]{2,1,0:T(8,128)(2,1)S(1)} %reshape.1659), channel_id=1, replica_groups=mesh['sp_0'=16,'sp_1'=2,'tp'=16] {'sp_0','sp_1'}, dimensions={0} | all-to-all | bytes 589824 | tf_op jit(solution)/shard_map/all_to_all | solution.py:249
  177.5 62.6 %all-gather.12.cloned.1.call-done = bf16[1,1152,2048]{2,1,0:T(8,128)(2,1)} async-done(((bf16[1,1152,128]{2,1,0:T(8,128)(2,1)}), bf16[1,1152,2048]{2,1,0:T(8,128)(2,1)}) %all-gather.12.cloned.1.call-update) | async-done | bytes 4718608 | tf_op jit(solution)/shard_map/all_gather | solution.py:250
  240.1 3.9 fusion.25
  244.1 2.4 fusion.34
  246.6 97.4 %all-gather.14.cloned.1.call-done = bf16[1152,4096]{1,0:T(8,128)(2,1)} async-done(((bf16[1152,256]{1,0:T(8,128)(2,1)}), bf16[1152,4096]{1,0:T(8,128)(2,1)}) %all-gather.14.cloned.1.call-update) | async-done | bytes 9437200 | tf_op jit(solution)/shard_map/all_gather | solution.py:260
  344.0 6.5 %convolution_convert_fusion.1 = bf16[1152,128]{1,0:T(8,128)(2,1)S(1)} fusion(bf16[1152,4096]{1,0:T(8,128)(2,1)} %all-gather.14.cloned.1.call-done, bf16[1,4096,128]{2,1,0:T(8,128)(2,1)} %param.35), kind=kOutput, calls=%fused_computation.43 | convolution fusion | flops 1208107008 | bytes 10780672 | tf_op jit(solution)/shard_map/esf,efd->esd/dot_general | solution.py:258
  350.7 4.0 all_to_all.33
  354.6 1.0 copy.64
  355.6 12.3 %all-to-all-start.4 = ((bf16[16,2,1,36,128]{4,1,3,2,0:T(2,128)(2,1)}), bf16[16,2,1,36,128]{4,1,3,2,0:T(2,128)(2,1)S(1)}, u32[]{:S(2)}, u32[]{:S(2)}) async-start(bf16[16,2,1,36,128]{4,1,3,2,0:T(2,128)(2,1)} %copy.64), calls=%async_computation.4 | async-start | bytes 589824 | tf_op jit(solution)/shard_map/all_to_all | solution.py:109
  368.1 19.8 %all-to-all-done.4 = bf16[16,2,1,36,128]{4,1,3,2,0:T(2,128)(2,1)S(1)} async-done(((bf16[16,2,1,36,128]{4,1,3,2,0:T(2,128)(2,1)}), bf16[16,2,1,36,128]{4,1,3,2,0:T(2,128)(2,1)S(1)}, u32[]{:S(2)}, u32[]{:S(2)}) %all-to-all-start.4) | async-done | bytes 294944 | tf_op jit(solution)/shard_map/all_to_all | solution.py:109
  387.9 1.9 gather_fusion.1
  (204 shorter events, 17.9 us)
Async XLA Ops:
  6.5 233.5 %copy-start = (bf16[1,2048,256]{2,1,0:T(8,128)(2,1)S(1)}, bf16[1,2048,256]{2,1,0:T(8,128)(2,1)}, u32[]{:S(2)}) copy-start(bf16[1,2048,256]{2,1,0:T(8,128)(2,1)} %param.33) | copy-start | bytes 3145732
  10.9 44.1 %copy-start.3 = (bf16[192,128]{1,0:T(8,128)(2,1)S(1)}, bf16[192,128]{1,0:T(8,128)(2,1)}, u32[]{:S(2)}) copy-start(bf16[192,128]{1,0:T(8,128)(2,1)} %param.22) | copy-start | bytes 147460
  12.6 41.7 %copy-start.4 = (f32[3,64,1,128]{3,1,2,0:T(8,128)}, f32[3,64,1,128]{3,1,2,0:T(8,128)S(1)}, u32[]{:S(2)}) copy-start(f32[3,64,1,128]{3,1,2,0:T(8,128)S(1)} %get-tuple-element.81) | copy-start | bytes 294916
  14.5 40.9 %copy-start.7 = (bf16[2,129,128]{2,1,0:T(8,128)(2,1)}, bf16[2,129,128]{2,1,0:T(8,128)(2,1)S(1)}, u32[]{:S(2)}) copy-start(bf16[2,129,128]{2,1,0:T(8,128)(2,1)S(1)} %all-gather.5) | copy-start | bytes 198148
  14.5 40.9 %copy-start.19 = (f32[128]{0:T(128)}, f32[128]{0:T(128)S(1)}, u32[]{:S(2)}) copy-start(f32[128]{0:T(128)S(1)} %fusion.382) | copy-start | bytes 1540
  15.1 40.3 %copy-start.16 = (f32[128]{0:T(128)}, f32[128]{0:T(128)S(1)}, u32[]{:S(2)}) copy-start(f32[128]{0:T(128)S(1)} %get-tuple-element.212) | copy-start | bytes 1540
  58.3 2.6 copy-start.6
  58.3 33.5 %copy-start.12 = (f32[3,128]{1,0:T(4,128)S(1)}, f32[3,128]{1,0:T(4,128)}, u32[]{:S(2)}) copy-start(f32[3,128]{1,0:T(4,128)} %get-tuple-element.225) | copy-start | bytes 4612
  60.2 31.1 %copy-start.8 = (bf16[2,129,128]{2,1,0:T(8,128)(2,1)}, bf16[2,129,128]{2,1,0:T(8,128)(2,1)S(1)}, u32[]{:S(2)}) copy-start(bf16[2,129,128]{2,1,0:T(8,128)(2,1)S(1)} %all-gather.7) | copy-start | bytes 198148
  92.1 3.2 copy-start.11
  93.3 2.6 copy-start.10
  93.3 2.6 copy-start.17
  93.3 2.6 copy-start.20
  93.3 2.6 copy-start.21
  93.3 2.6 copy-start.22
  93.3 2.6 copy-start.23
  93.4 2.6 copy-start.24
  93.4 2.6 copy-start.25
  93.4 2.6 copy-start.26
  93.4 2.6 copy-start.27
  93.4 2.6 copy-start.28
  93.4 2.6 copy-start.29
  98.1 8.7 %copy-start.13 = (s32[192,4]{0,1:T(4,128)S(1)}, s32[192,4]{0,1:T(4,128)}, u32[]{:S(2)}) copy-start(s32[192,4]{0,1:T(4,128)} %param.31) | copy-start | bytes 9220
  99.3 19.4 %all-to-all-start = ((bf16[16,12,2048]{2,1,0:T(8,128)(2,1)}), bf16[16,12,2048]{2,1,0:T(8,128)(2,1)S(1)}, u32[]{:S(2)}, u32[]{:S(2)}) async-start(bf16[16,12,2048]{2,1,0:T(8,128)(2,1)} %reshape.1657), calls=%async_computation | async-start | bytes 2097152 | tf_op jit(solution)/shard_map/all_to_all | solution.py:72
  120.0 17.0 %all-to-all-start.1 = ((bf16[16,12,2048]{2,1,0:T(8,128)(2,1)}), bf16[16,12,2048]{2,1,0:T(8,128)(2,1)S(1)}, u32[]{:S(2)}, u32[]{:S(2)}) async-start(bf16[16,12,2048]{2,1,0:T(8,128)(2,1)} %broadcast_in_dim.35), calls=%async_computation.1 | async-start | bytes 2097152 | tf_op jit(solution)/shard_map/all_to_all | solution.py:91
  124.9 115.1 %all-gather.12.cloned.1.call-start = ((), (), s32[]{:S(2)}) async-start(), calls=%async_computation.5 | async-start | bytes 5013504 | tf_op jit(solution)/shard_map/all_gather | solution.py:250
  125.2 13.1 %copy-start.1 = (bf16[192,2048]{1,0:T(8,128)(2,1)S(1)}, bf16[192,2048]{1,0:T(8,128)(2,1)}, u32[]{:S(2)}) copy-start(bf16[192,2048]{1,0:T(8,128)(2,1)} %param.20) | copy-start | bytes 2359300
  177.3 166.7 %all-gather.14.cloned.1.call-start = ((), (), s32[]{:S(2)}) async-start(), calls=%async_computation.6 | async-start | bytes 10027008 | tf_op jit(solution)/shard_map/all_gather | solution.py:260
  240.1 3.9 copy-start.37
  240.1 4.1 %copy-start.38 = (bf16[1,2048,256]{2,1,0:T(8,128)(2,1)S(1)}, bf16[1,2048,256]{2,1,0:T(8,128)(2,1)}, u32[]{:S(2)}) copy-start(bf16[1,2048,256]{2,1,0:T(8,128)(2,1)} %param.34) | copy-start | bytes 3145732
  350.5 17.4 %copy-start.15 = (f32[192,4]{0,1:T(4,128)S(1)}, f32[192,4]{0,1:T(4,128)}, u32[]{:S(2)}) copy-start(f32[192,4]{0,1:T(4,128)} %param.32) | copy-start | bytes 9220
  355.6 32.2 %all-to-all-start.4 = ((bf16[16,2,1,36,128]{4,1,3,2,0:T(2,128)(2,1)}), bf16[16,2,1,36,128]{4,1,3,2,0:T(2,128)(2,1)S(1)}, u32[]{:S(2)}, u32[]{:S(2)}) async-start(bf16[16,2,1,36,128]{4,1,3,2,0:T(2,128)(2,1)} %copy.64), calls=%async_computation.4 | async-start | bytes 589824 | tf_op jit(solution)/shard_map/all_to_all | solution.py:109
  (13 other events, 31.5 us)
Sparse Core Ops, SparseCore 0:
  177.4 62.6 all-gather.11
  246.7 97.2 all-gather.13
where the time goes:
time: 398 us
  waiting for transfers between devices  197 us (49%)
  blocking collectives  108 us (27%)
  starting transfers between devices  25 us (6%)
  matrix products  21.1 us (5%)
  local copies, waits for them, and re-layouts  18.4 us (5%)
  between operations  14.5 us (4%)
  other arithmetic  12.4 us (3%)
    all_gather x1, waiting for transfers between devices, shards(): lax.all_gather(active, 'tp', axis=2, tiled=True)  97.4 us
    all_gather x4, blocking collectives, all_in_one(): both, at, found = (lax.all_gather(jnp.concatenate(lines), axis), 0, {})  71.3 us
    all_gather x1, waiting for transfers between devices, shards(): piece = lax.all_gather(arrived, 'tp', axis=2, tiled=True)  62.6 us
    all_to_all x1, blocking collectives, shards(): lax.all_to_all(buffer, SP, split_axis=0, concat_axis=1, tiled=True)  33.2 us
    all_to_all x1, waiting for transfers between devices, turned_blocks(): filled = lax.all_to_all(filled, axes[k], k, k, tiled=True)  19.8 us
    all_to_all x1, starting transfers between devices, turned_blocks(): filled = lax.all_to_all(filled, axes[k], k, k, tiled=True)  12.3 us
    all_to_all x1, waiting for transfers between devices, sent_and_summed(): pieces = lax.all_to_all(in_blocks(x, dim, length), axis, 0, 0, tiled=True)  9.91 us
  transfers between devices with their start and end apart: 5, of which 5 were waited for; matrix products, arithmetic and copies ran while one was open for 2% of the time, Pallas kernels for 0%

commit v1 on v0

--- a/solution.py
+++ b/solution.py
@@ -1,3 +1,4 @@
+import functools
 import math
 import jax
 import jax.numpy as jnp
@@ -12,6 +13,33 @@
 eps_norm = 1e-06
 limit_value = 7.0
 alpha_value = 1.702
+
+
+def take_cards(u, axis_id):
+    chips = jax.lax.axis_size(axis_id)
+    src_i = 0
+    kept_rows = []
+    while src_i < chips:
+        kept_rows.append((src_i, (src_i + 1) % chips))
+        src_i = src_i + 1
+    src_i = 0
+    fields = []
+    while src_i < chips:
+        fields.append((src_i, (src_i - 1) % chips))
+        src_i += 1
+    b_now, current_block = ([u], [u])
+    for _ in range(chips // 2):
+        b_now.append(jax.lax.ppermute(b_now[-1], axis_name=axis_id, perm=kept_rows))
+    p = 0
+    while p < (chips - 1) // 2:
+        current_block.append(jax.lax.ppermute(current_block[-1], axis_id, perm=fields))
+        p += 1
+    w_next = jnp.concatenate([*b_now[::-1], *current_block[1:]], axis=2)
+    z1 = jnp.roll(w_next, (jax.lax.axis_index(axis_id) - chips // 2) * u.shape[2], 2)
+    return z1
+
+
+spread_limits = functools.partial(take_cards, axis_id="tp")
 
 
 def filled_with(x, identity):
@@ -256,10 +284,7 @@
         jnp.bfloat16
     )
     produced = jnp.einsum(
-        "esf,efd->esd",
-        lax.all_gather(active, "tp", axis=2, tiled=True),
-        w_down,
-        preferred_element_type=jnp.float32,
+        "esf,efd->esd", spread_limits(active), w_down, preferred_element_type=jnp.float32
     ).astype(jnp.bfloat16)
     returned = core_and_chips(produced, ("sp_0", "sp_1"), (1, 0), 1, 0)
     picked = returned.reshape(EXPERTS * CAP, part_width)[slot_index].astype(jnp.float32)

time: 398 us -> 458 us (1.15)
  the two profiles are of different devices: /device:TPU:2 before, /device:TPU:32 now
where the time goes in v1:
time: 458 us; the launch traced here: 456 us
  waiting for transfers between devices  164 us (36%)
  blocking collectives  106 us (23%)
  starting transfers between devices  91.8 us (20%)
  local copies, waits for them, and re-layouts  42.1 us (9%)
  matrix products  21.7 us (5%)
  between operations  14.7 us (3%)
  other arithmetic  14.5 us (3%)
    all_gather x4, blocking collectives, all_in_one(): both, at, found = (lax.all_gather(jnp.concatenate(lines), axis), 0, {})  71.1 us
    all_gather x1, waiting for transfers between devices, shards(): piece = lax.all_gather(arrived, 'tp', axis=2, tiled=True)  63.8 us
    ppermute x8, waiting for transfers between devices, take_cards(): b_now.append(jax.lax.ppermute(b_now[-1], axis_name=axis_id, perm=kept_rows))  61.1 us
    ppermute x7, starting transfers between devices, take_cards(): jax.lax.ppermute(current_block[-1], axis_id, perm=fields)  52 us
    all_to_all x1, blocking collectives, shards(): lax.all_to_all(buffer, SP, split_axis=0, concat_axis=1, tiled=True)  31.4 us
    unnamed x103, local copies, waits for them, and re-layouts  23.5 us
    all_to_all x1, waiting for transfers between devices, turned_blocks(): filled = lax.all_to_all(filled, axes[k], k, k, tiled=True)  19 us
    ppermute x8, starting transfers between devices, take_cards(): b_now.append(jax.lax.ppermute(b_now[-1], axis_name=axis_id, perm=kept_rows))  16.4 us
  transfers between devices with their start and end apart: 19, of which 14 were waited for; matrix products, arithmetic and copies ran while one was open for 5% of the time, Pallas kernels for 0%

profile of v1, /device:TPU:32, one launch (start us, length us, event | category | flops | bytes accessed | tf_op | source)
XLA Modules:
  0.0 455.5 jit_solution(5578979661529291351)
XLA Ops:
  14.7 36.5 %all-gather.5 = bf16[16,129,128]{2,1,0:T(8,128)(2,1)S(1)} all-gather(bf16[1,129,128]{2,1,0:T(8,128)(2,1)S(1)} %maximum_bitcast_fusion.1), channel_id=3, replica_groups=mesh['sp_0'=16,'sp_1'=2,'tp'=16] {'sp_0'}, dimensions={0}, use_global_device_ids=true | all-gather | bytes 561408 | tf_op jit(solution)/shard_map/all_gather | solution.py:59
  59.0 30.9 %all-gather.7 = bf16[16,129,128]{2,1,0:T(8,128)(2,1)S(1)} all-gather(bf16[1,129,128]{2,1,0:T(8,128)(2,1)S(1)} %maximum_bitcast_fusion.3), channel_id=5, replica_groups=mesh['sp_0'=16,'sp_1'=2,'tp'=16] {'sp_0'}, dimensions={0}, use_global_device_ids=true | all-gather | bytes 561408 | tf_op jit(solution)/shard_map/all_gather | solution.py:59
  103.5 7.0 %all-to-all-start = ((bf16[16,12,2048]{2,1,0:T(8,128)(2,1)}), bf16[16,12,2048]{2,1,0:T(8,128)(2,1)S(1)}, u32[]{:S(2)}, u32[]{:S(2)}) async-start(bf16[16,12,2048]{2,1,0:T(8,128)(2,1)} %reshape.1657), calls=%async_computation | async-start | bytes 2097152 | tf_op jit(solution)/shard_map/all_to_all | solution.py:100
  113.9 10.0 %all-to-all-done = bf16[16,12,2048]{2,1,0:T(8,128)(2,1)S(1)} async-done(((bf16[16,12,2048]{2,1,0:T(8,128)(2,1)}), bf16[16,12,2048]{2,1,0:T(8,128)(2,1)S(1)}, u32[]{:S(2)}, u32[]{:S(2)}) %all-to-all-start) | async-done | bytes 786464 | tf_op jit(solution)/shard_map/all_to_all | solution.py:100
  125.2 3.7 all-to-all-start.1
  129.7 3.4 scatter_custom_fusion
  133.1 9.1 %all-to-all-done.1 = bf16[16,12,2048]{2,1,0:T(8,128)(2,1)S(1)} async-done(((bf16[16,12,2048]{2,1,0:T(8,128)(2,1)}), bf16[16,12,2048]{2,1,0:T(8,128)(2,1)S(1)}, u32[]{:S(2)}, u32[]{:S(2)}) %all-to-all-start.1) | async-done | bytes 786464 | tf_op jit(solution)/shard_map/all_to_all | solution.py:119
  145.4 2.9 gather_fusion
  148.4 31.4 %all_to_all.32 = bf16[32,36,128]{2,1,0:T(8,128)(2,1)S(1)} all-to-all(bf16[32,36,128]{2,1,0:T(8,128)(2,1)S(1)} %reshape.1659), channel_id=1, replica_groups=mesh['sp_0'=16,'sp_1'=2,'tp'=16] {'sp_0','sp_1'}, dimensions={0} | all-to-all | bytes 589824 | tf_op jit(solution)/shard_map/all_to_all | solution.py:277
  180.6 63.8 %all-gather.10.cloned.1.call-done = bf16[1,1152,2048]{2,1,0:T(8,128)(2,1)} async-done(((bf16[1,1152,128]{2,1,0:T(8,128)(2,1)}), bf16[1,1152,2048]{2,1,0:T(8,128)(2,1)}) %all-gather.10.cloned.1.call-update) | async-done | bytes 4718608 | tf_op jit(solution)/shard_map/all_gather | solution.py:278
  244.4 3.9 fusion.28
  248.3 4.4 fusion.40
  252.7 3.1 collective-permute-start
  255.8 15.8 %collective-permute-done = bf16[1,1152,256]{1,2,0:T(8,128)(2,1)S(1)} collective-permute-done((bf16[1,1152,256]{1,2,0:T(8,128)(2,1)S(1)}, bf16[1,1152,256]{1,2,0:T(8,128)(2,1)S(1)}, u32[]{:S(2)}, u32[]{:S(2)}) %collective-permute-start) | collective-permute-done | bytes 589856 | tf_op jit(solution)/shard_map/ppermute | solution.py:32
  273.6 7.2 %collective-permute-start.8 = (bf16[1,1152,256]{1,2,0:T(8,128)(2,1)S(1)}, bf16[1,1152,256]{1,2,0:T(8,128)(2,1)S(1)}, u32[]{:S(2)}, u32[]{:S(2)}) collective-permute-start(bf16[1,1152,256]{1,2,0:T(8,128)(2,1)S(1)} %fusion.40), channel_id=1, source_target_pairs={{0,15},{1,0},{2,1},{3,2},{4,3},{5,4},{6,5},{7,6},{8,7},{9,8},{10,9... | collective-permute-start | bytes 1769480 | tf_op jit(solution)/shard_map/ppermute | solution.py:35
  280.8 8.9 %collective-permute-done.1 = bf16[1,1152,256]{1,2,0:T(8,128)(2,1)S(1)} collective-permute-done((bf16[1,1152,256]{1,2,0:T(8,128)(2,1)S(1)}, bf16[1,1152,256]{1,2,0:T(8,128)(2,1)S(1)}, u32[]{:S(2)}, u32[]{:S(2)}) %collective-permute-start.1) | collective-permute-done | bytes 589856 | tf_op jit(solution)/shard_map/ppermute | solution.py:32
  291.6 7.2 %collective-permute-start.9 = (bf16[1,1152,256]{1,2,0:T(8,128)(2,1)S(1)}, bf16[1,1152,256]{1,2,0:T(8,128)(2,1)S(1)}, u32[]{:S(2)}, u32[]{:S(2)}) collective-permute-start(bf16[1,1152,256]{1,2,0:T(8,128)(2,1)S(1)} %collective-permute-done.8), channel_id=1, source_target_pairs={{0,15},{1,0},{2,1},{3,2},{4,3},{5,4},{6,5},{7,6},{8,7},{9,8},{10,9... | collective-permute-start | bytes 1769480 | tf_op jit(solution)/shard_map/ppermute | solution.py:35
  298.9 8.0 %collective-permute-done.2 = bf16[1,1152,256]{1,2,0:T(8,128)(2,1)S(1)} collective-permute-done((bf16[1,1152,256]{1,2,0:T(8,128)(2,1)S(1)}, bf16[1,1152,256]{1,2,0:T(8,128)(2,1)S(1)}, u32[]{:S(2)}, u32[]{:S(2)}) %collective-permute-start.2) | collective-permute-done | bytes 589856 | tf_op jit(solution)/shard_map/ppermute | solution.py:32
  308.8 7.2 %collective-permute-start.10 = (bf16[1,1152,256]{1,2,0:T(8,128)(2,1)S(1)}, bf16[1,1152,256]{1,2,0:T(8,128)(2,1)S(1)}, u32[]{:S(2)}, u32[]{:S(2)}) collective-permute-start(bf16[1,1152,256]{1,2,0:T(8,128)(2,1)S(1)} %collective-permute-done.9), channel_id=1, source_target_pairs={{0,15},{1,0},{2,1},{3,2},{4,3},{5,4},{6,5},{7,6},{8,7},{9,8},{10,9... | collective-permute-start | bytes 1769480 | tf_op jit(solution)/shard_map/ppermute | solution.py:35
  316.1 7.1 %collective-permute-done.3 = bf16[1,1152,256]{1,2,0:T(8,128)(2,1)S(1)} collective-permute-done((bf16[1,1152,256]{1,2,0:T(8,128)(2,1)S(1)}, bf16[1,1152,256]{1,2,0:T(8,128)(2,1)S(1)}, u32[]{:S(2)}, u32[]{:S(2)}) %collective-permute-start.3) | collective-permute-done | bytes 589856 | tf_op jit(solution)/shard_map/ppermute | solution.py:32
  325.2 7.2 %collective-permute-start.11 = (bf16[1,1152,256]{1,2,0:T(8,128)(2,1)S(1)}, bf16[1,1152,256]{1,2,0:T(8,128)(2,1)S(1)}, u32[]{:S(2)}, u32[]{:S(2)}) collective-permute-start(bf16[1,1152,256]{1,2,0:T(8,128)(2,1)S(1)} %collective-permute-done.10), channel_id=1, source_target_pairs={{0,15},{1,0},{2,1},{3,2},{4,3},{5,4},{6,5},{7,6},{8,7},{9,8},{10,9... | collective-permute-start | bytes 1769480 | tf_op jit(solution)/shard_map/ppermute | solution.py:35
  332.4 6.3 %collective-permute-done.4 = bf16[1,1152,256]{1,2,0:T(8,128)(2,1)S(1)} collective-permute-done((bf16[1,1152,256]{1,2,0:T(8,128)(2,1)S(1)}, bf16[1,1152,256]{1,2,0:T(8,128)(2,1)S(1)}, u32[]{:S(2)}, u32[]{:S(2)}) %collective-permute-start.4) | collective-permute-done | bytes 589856 | tf_op jit(solution)/shard_map/ppermute | solution.py:32
  341.5 7.2 %collective-permute-start.12 = (bf16[1,1152,256]{1,2,0:T(8,128)(2,1)S(1)}, bf16[1,1152,256]{1,2,0:T(8,128)(2,1)}, u32[]{:S(2)}, u32[]{:S(2)}) collective-permute-start(bf16[1,1152,256]{1,2,0:T(8,128)(2,1)S(1)} %collective-permute-done.11), channel_id=1, source_target_pairs={{0,15},{1,0},{2,1},{3,2},{4,3},{5,4},{6,5},{7,6},{8,7},{9,8},{10,9... | collective-permute-start | bytes 1769480 | tf_op jit(solution)/shard_map/ppermute | solution.py:35
  348.7 5.1 %collective-permute-done.5 = bf16[1,1152,256]{1,2,0:T(8,128)(2,1)S(1)} collective-permute-done((bf16[1,1152,256]{1,2,0:T(8,128)(2,1)S(1)}, bf16[1,1152,256]{1,2,0:T(8,128)(2,1)S(1)}, u32[]{:S(2)}, u32[]{:S(2)}) %collective-permute-start.5) | collective-permute-done | bytes 589856 | tf_op jit(solution)/shard_map/ppermute | solution.py:32
  356.1 7.8 %collective-permute-start.13 = (bf16[1,1152,256]{1,2,0:T(8,128)(2,1)}, bf16[1,1152,256]{1,2,0:T(8,128)(2,1)}, u32[]{:S(2)}, u32[]{:S(2)}) collective-permute-start(bf16[1,1152,256]{1,2,0:T(8,128)(2,1)} %collective-permute-done.12), channel_id=1, source_target_pairs={{0,15},{1,0},{2,1},{3,2},{4,3},{5,4},{6,5},{7,6},{8,7},{9,8},{10,9... | collective-permute-start | bytes 1769480 | tf_op jit(solution)/shard_map/ppermute | solution.py:35
  363.9 5.1 %collective-permute-done.6 = bf16[1,1152,256]{1,2,0:T(8,128)(2,1)} collective-permute-done((bf16[1,1152,256]{1,2,0:T(8,128)(2,1)S(1)}, bf16[1,1152,256]{1,2,0:T(8,128)(2,1)}, u32[]{:S(2)}, u32[]{:S(2)}) %collective-permute-start.6) | collective-permute-done | bytes 589856 | tf_op jit(solution)/shard_map/ppermute | solution.py:32
  371.6 8.0 %collective-permute-start.14 = (bf16[1,1152,256]{1,2,0:T(8,128)(2,1)}, bf16[1,1152,256]{1,2,0:T(8,128)(2,1)S(1)}, u32[]{:S(2)}, u32[]{:S(2)}) collective-permute-start(bf16[1,1152,256]{1,2,0:T(8,128)(2,1)} %collective-permute-done.13), channel_id=1, source_target_pairs={{0,15},{1,0},{2,1},{3,2},{4,3},{5,4},{6,5},{7,6},{8,7},{9,8},{10,9... | collective-permute-start | bytes 1769480 | tf_op jit(solution)/shard_map/ppermute | solution.py:35
  379.6 4.8 %collective-permute-done.7 = bf16[1,1152,256]{1,2,0:T(8,128)(2,1)} collective-permute-done((bf16[1,1152,256]{1,2,0:T(8,128)(2,1)}, bf16[1,1152,256]{1,2,0:T(8,128)(2,1)}, u32[]{:S(2)}, u32[]{:S(2)}) %collective-permute-start.7) | collective-permute-done | bytes 589856 | tf_op jit(solution)/shard_map/ppermute | solution.py:32
  406.1 2.7 fusion.43
  408.9 4.0 all_to_all.33
  413.9 12.7 %all-to-all-start.4 = ((bf16[16,2,1,36,128]{4,1,3,2,0:T(2,128)(2,1)}), bf16[16,2,1,36,128]{4,1,3,2,0:T(2,128)(2,1)S(1)}, u32[]{:S(2)}, u32[]{:S(2)}) async-start(bf16[16,2,1,36,128]{4,1,3,2,0:T(2,128)(2,1)} %copy.64), calls=%async_computation.4 | async-start | bytes 589824 | tf_op jit(solution)/shard_map/all_to_all | solution.py:137
  426.7 19.0 %all-to-all-done.4 = bf16[16,2,1,36,128]{4,1,3,2,0:T(2,128)(2,1)S(1)} async-done(((bf16[16,2,1,36,128]{4,1,3,2,0:T(2,128)(2,1)}), bf16[16,2,1,36,128]{4,1,3,2,0:T(2,128)(2,1)S(1)}, u32[]{:S(2)}, u32[]{:S(2)}) %all-to-all-start.4) | async-done | bytes 294944 | tf_op jit(solution)/shard_map/all_to_all | solution.py:137
  (251 shorter events, 82.5 us)
Async XLA Ops:
  6.5 237.9 %copy-start = (bf16[1,2048,256]{2,1,0:T(8,128)(2,1)S(1)}, bf16[1,2048,256]{2,1,0:T(8,128)(2,1)}, u32[]{:S(2)}) copy-start(bf16[1,2048,256]{2,1,0:T(8,128)(2,1)} %param.33) | copy-start | bytes 3145732
  6.5 136.9 %copy-start.21 = (bf16[192,2048]{1,0:T(8,128)(2,1)S(1)}, bf16[192,2048]{1,0:T(8,128)(2,1)}, u32[]{:S(2)}) copy-start(bf16[192,2048]{1,0:T(8,128)(2,1)} %param.20) | copy-start | bytes 2359300
  12.1 39.8 %copy-start.23 = (f32[3,64,1,128]{3,1,2,0:T(8,128)}, f32[3,64,1,128]{3,1,2,0:T(8,128)S(1)}, u32[]{:S(2)}) copy-start(f32[3,64,1,128]{3,1,2,0:T(8,128)S(1)} %get-tuple-element.81) | copy-start | bytes 294916
  14.0 39.8 %copy-start.25 = (bf16[2,129,128]{2,1,0:T(8,128)(2,1)}, bf16[2,129,128]{2,1,0:T(8,128)(2,1)S(1)}, u32[]{:S(2)}) copy-start(bf16[2,129,128]{2,1,0:T(8,128)(2,1)S(1)} %all-gather.4) | copy-start | bytes 198148
  14.0 39.8 %copy-start.31 = (f32[128]{0:T(128)}, f32[128]{0:T(128)S(1)}, u32[]{:S(2)}) copy-start(f32[128]{0:T(128)S(1)} %fusion.392) | copy-start | bytes 1540
  14.5 39.2 %copy-start.29 = (f32[128]{0:T(128)}, f32[128]{0:T(128)S(1)}, u32[]{:S(2)}) copy-start(f32[128]{0:T(128)S(1)} %get-tuple-element.212) | copy-start | bytes 1540
  93.5 51.7 %copy-start.27 = (f32[2048]{0:T(1024)S(1)}, f32[2048]{0:T(1024)}, u32[]{:S(2)}) copy-start(f32[2048]{0:T(1024)} %param.30) | copy-start | bytes 24580
  103.5 20.4 %all-to-all-start = ((bf16[16,12,2048]{2,1,0:T(8,128)(2,1)}), bf16[16,12,2048]{2,1,0:T(8,128)(2,1)S(1)}, u32[]{:S(2)}, u32[]{:S(2)}) async-start(bf16[16,12,2048]{2,1,0:T(8,128)(2,1)} %reshape.1657), calls=%async_computation | async-start | bytes 2097152 | tf_op jit(solution)/shard_map/all_to_all | solution.py:100
  125.2 17.0 %all-to-all-start.1 = ((bf16[16,12,2048]{2,1,0:T(8,128)(2,1)}), bf16[16,12,2048]{2,1,0:T(8,128)(2,1)S(1)}, u32[]{:S(2)}, u32[]{:S(2)}) async-start(bf16[16,12,2048]{2,1,0:T(8,128)(2,1)} %broadcast_in_dim.35), calls=%async_computation.1 | async-start | bytes 2097152 | tf_op jit(solution)/shard_map/all_to_all | solution.py:119
  128.8 115.6 %all-gather.10.cloned.1.call-start = ((), (), s32[]{:S(2)}) async-start(), calls=%async_computation.5 | async-start | bytes 5013504 | tf_op jit(solution)/shard_map/all_gather | solution.py:278
  252.7 18.9 %collective-permute-start = (bf16[1,1152,256]{1,2,0:T(8,128)(2,1)S(1)}, bf16[1,1152,256]{1,2,0:T(8,128)(2,1)S(1)}, u32[]{:S(2)}, u32[]{:S(2)}) collective-permute-start(bf16[1,1152,256]{1,2,0:T(8,128)(2,1)S(1)} %fusion.40), channel_id=1, source_target_pairs={{0,1},{1,2},{2,3},{3,4},{4,5},{5,6},{6,7},{7,8},{8,9},{9,10},{10,1... | collective-permute-start | bytes 1769480 | tf_op jit(solution)/shard_map/ppermute | solution.py:32
  271.6 18.0 %collective-permute-start.1 = (bf16[1,1152,256]{1,2,0:T(8,128)(2,1)S(1)}, bf16[1,1152,256]{1,2,0:T(8,128)(2,1)S(1)}, u32[]{:S(2)}, u32[]{:S(2)}) collective-permute-start(bf16[1,1152,256]{1,2,0:T(8,128)(2,1)S(1)} %collective-permute-done), channel_id=1, source_target_pairs={{0,1},{1,2},{2,3},{3,4},{4,5},{5,6},{6,7},{7,8},{8,9},{9,10},{10,1... | collective-permute-start | bytes 1769480 | tf_op jit(solution)/shard_map/ppermute | solution.py:32
  273.6 18.1 %collective-permute-start.8 = (bf16[1,1152,256]{1,2,0:T(8,128)(2,1)S(1)}, bf16[1,1152,256]{1,2,0:T(8,128)(2,1)S(1)}, u32[]{:S(2)}, u32[]{:S(2)}) collective-permute-start(bf16[1,1152,256]{1,2,0:T(8,128)(2,1)S(1)} %fusion.40), channel_id=1, source_target_pairs={{0,15},{1,0},{2,1},{3,2},{4,3},{5,4},{6,5},{7,6},{8,7},{9,8},{10,9... | collective-permute-start | bytes 1769480 | tf_op jit(solution)/shard_map/ppermute | solution.py:35
  289.7 17.2 %collective-permute-start.2 = (bf16[1,1152,256]{1,2,0:T(8,128)(2,1)S(1)}, bf16[1,1152,256]{1,2,0:T(8,128)(2,1)S(1)}, u32[]{:S(2)}, u32[]{:S(2)}) collective-permute-start(bf16[1,1152,256]{1,2,0:T(8,128)(2,1)S(1)} %collective-permute-done.1), channel_id=1, source_target_pairs={{0,1},{1,2},{2,3},{3,4},{4,5},{5,6},{6,7},{7,8},{8,9},{9,10},{10,1... | collective-permute-start | bytes 1769480 | tf_op jit(solution)/shard_map/ppermute | solution.py:32
  291.6 17.2 %collective-permute-start.9 = (bf16[1,1152,256]{1,2,0:T(8,128)(2,1)S(1)}, bf16[1,1152,256]{1,2,0:T(8,128)(2,1)S(1)}, u32[]{:S(2)}, u32[]{:S(2)}) collective-permute-start(bf16[1,1152,256]{1,2,0:T(8,128)(2,1)S(1)} %collective-permute-done.8), channel_id=1, source_target_pairs={{0,15},{1,0},{2,1},{3,2},{4,3},{5,4},{6,5},{7,6},{8,7},{9,8},{10,9... | collective-permute-start | bytes 1769480 | tf_op jit(solution)/shard_map/ppermute | solution.py:35
  306.9 16.3 %collective-permute-start.3 = (bf16[1,1152,256]{1,2,0:T(8,128)(2,1)S(1)}, bf16[1,1152,256]{1,2,0:T(8,128)(2,1)S(1)}, u32[]{:S(2)}, u32[]{:S(2)}) collective-permute-start(bf16[1,1152,256]{1,2,0:T(8,128)(2,1)S(1)} %collective-permute-done.2), channel_id=1, source_target_pairs={{0,1},{1,2},{2,3},{3,4},{4,5},{5,6},{6,7},{7,8},{8,9},{9,10},{10,1... | collective-permute-start | bytes 1769480 | tf_op jit(solution)/shard_map/ppermute | solution.py:32
  308.8 16.3 %collective-permute-start.10 = (bf16[1,1152,256]{1,2,0:T(8,128)(2,1)S(1)}, bf16[1,1152,256]{1,2,0:T(8,128)(2,1)S(1)}, u32[]{:S(2)}, u32[]{:S(2)}) collective-permute-start(bf16[1,1152,256]{1,2,0:T(8,128)(2,1)S(1)} %collective-permute-done.9), channel_id=1, source_target_pairs={{0,15},{1,0},{2,1},{3,2},{4,3},{5,4},{6,5},{7,6},{8,7},{9,8},{10,9... | collective-permute-start | bytes 1769480 | tf_op jit(solution)/shard_map/ppermute | solution.py:35
  323.2 32.9 %copy-start.15 = (bf16[1,1152,256]{1,2,0:T(8,128)(2,1)}, bf16[1,1152,256]{1,2,0:T(8,128)(2,1)S(1)}, u32[]{:S(2)}) copy-start(bf16[1,1152,256]{1,2,0:T(8,128)(2,1)S(1)} %collective-permute-done.3) | copy-start | bytes 1769476
  323.2 15.5 %collective-permute-start.4 = (bf16[1,1152,256]{1,2,0:T(8,128)(2,1)S(1)}, bf16[1,1152,256]{1,2,0:T(8,128)(2,1)S(1)}, u32[]{:S(2)}, u32[]{:S(2)}) collective-permute-start(bf16[1,1152,256]{1,2,0:T(8,128)(2,1)S(1)} %collective-permute-done.3), channel_id=1, source_target_pairs={{0,1},{1,2},{2,3},{3,4},{4,5},{5,6},{6,7},{7,8},{8,9},{9,10},{10,1... | collective-permute-start | bytes 1769480 | tf_op jit(solution)/shard_map/ppermute | solution.py:32
  325.2 15.5 %collective-permute-start.11 = (bf16[1,1152,256]{1,2,0:T(8,128)(2,1)S(1)}, bf16[1,1152,256]{1,2,0:T(8,128)(2,1)S(1)}, u32[]{:S(2)}, u32[]{:S(2)}) collective-permute-start(bf16[1,1152,256]{1,2,0:T(8,128)(2,1)S(1)} %collective-permute-done.10), channel_id=1, source_target_pairs={{0,15},{1,0},{2,1},{3,2},{4,3},{5,4},{6,5},{7,6},{8,7},{9,8},{10,9... | collective-permute-start | bytes 1769480 | tf_op jit(solution)/shard_map/ppermute | solution.py:35
  338.7 15.1 %collective-permute-start.5 = (bf16[1,1152,256]{1,2,0:T(8,128)(2,1)S(1)}, bf16[1,1152,256]{1,2,0:T(8,128)(2,1)S(1)}, u32[]{:S(2)}, u32[]{:S(2)}) collective-permute-start(bf16[1,1152,256]{1,2,0:T(8,128)(2,1)S(1)} %collective-permute-done.4), channel_id=1, source_target_pairs={{0,1},{1,2},{2,3},{3,4},{4,5},{5,6},{6,7},{7,8},{8,9},{9,10},{10,1... | collective-permute-start | bytes 1769480 | tf_op jit(solution)/shard_map/ppermute | solution.py:32
  341.5 14.6 %collective-permute-start.12 = (bf16[1,1152,256]{1,2,0:T(8,128)(2,1)S(1)}, bf16[1,1152,256]{1,2,0:T(8,128)(2,1)}, u32[]{:S(2)}, u32[]{:S(2)}) collective-permute-start(bf16[1,1152,256]{1,2,0:T(8,128)(2,1)S(1)} %collective-permute-done.11), channel_id=1, source_target_pairs={{0,15},{1,0},{2,1},{3,2},{4,3},{5,4},{6,5},{7,6},{8,7},{9,8},{10,9... | collective-permute-start | bytes 1769480 | tf_op jit(solution)/shard_map/ppermute | solution.py:35
  353.8 15.2 %collective-permute-start.6 = (bf16[1,1152,256]{1,2,0:T(8,128)(2,1)S(1)}, bf16[1,1152,256]{1,2,0:T(8,128)(2,1)}, u32[]{:S(2)}, u32[]{:S(2)}) collective-permute-start(bf16[1,1152,256]{1,2,0:T(8,128)(2,1)S(1)} %collective-permute-done.5), channel_id=1, source_target_pairs={{0,1},{1,2},{2,3},{3,4},{4,5},{5,6},{6,7},{7,8},{8,9},{9,10},{10,1... | collective-permute-start | bytes 1769480 | tf_op jit(solution)/shard_map/ppermute | solution.py:32
  356.1 15.5 %collective-permute-start.13 = (bf16[1,1152,256]{1,2,0:T(8,128)(2,1)}, bf16[1,1152,256]{1,2,0:T(8,128)(2,1)}, u32[]{:S(2)}, u32[]{:S(2)}) collective-permute-start(bf16[1,1152,256]{1,2,0:T(8,128)(2,1)} %collective-permute-done.12), channel_id=1, source_target_pairs={{0,15},{1,0},{2,1},{3,2},{4,3},{5,4},{6,5},{7,6},{8,7},{9,8},{10,9... | collective-permute-start | bytes 1769480 | tf_op jit(solution)/shard_map/ppermute | solution.py:35
  369.0 15.4 %collective-permute-start.7 = (bf16[1,1152,256]{1,2,0:T(8,128)(2,1)}, bf16[1,1152,256]{1,2,0:T(8,128)(2,1)}, u32[]{:S(2)}, u32[]{:S(2)}) collective-permute-start(bf16[1,1152,256]{1,2,0:T(8,128)(2,1)} %collective-permute-done.6), channel_id=1, source_target_pairs={{0,1},{1,2},{2,3},{3,4},{4,5},{5,6},{6,7},{7,8},{8,9},{9,10},{10,1... | collective-permute-start | bytes 1769480 | tf_op jit(solution)/shard_map/ppermute | solution.py:32
  371.0 32.4 %copy-start.4 = (bf16[1,1152,256]{1,2,0:T(8,128)(2,1)S(1)}, bf16[1,1152,256]{1,2,0:T(8,128)(2,1)}, u32[]{:S(2)}) copy-start(bf16[1,1152,256]{1,2,0:T(8,128)(2,1)} %copy-done.3) | copy-start | bytes 1769476
  371.0 32.4 %copy-start.8 = (bf16[1,1152,256]{1,2,0:T(8,128)(2,1)S(1)}, bf16[1,1152,256]{1,2,0:T(8,128)(2,1)}, u32[]{:S(2)}) copy-start(bf16[1,1152,256]{1,2,0:T(8,128)(2,1)} %copy-done.7) | copy-start | bytes 1769476
  371.0 32.5 %copy-start.12 = (bf16[1,1152,256]{1,2,0:T(8,128)(2,1)S(1)}, bf16[1,1152,256]{1,2,0:T(8,128)(2,1)}, u32[]{:S(2)}) copy-start(bf16[1,1152,256]{1,2,0:T(8,128)(2,1)} %copy-done.11) | copy-start | bytes 1769476
  371.0 32.6 %copy-start.14 = (bf16[1,1152,256]{1,2,0:T(8,128)(2,1)S(1)}, bf16[1,1152,256]{1,2,0:T(8,128)(2,1)}, u32[]{:S(2)}) copy-start(bf16[1,1152,256]{1,2,0:T(8,128)(2,1)} %copy-done.13) | copy-start | bytes 1769476
  371.0 35.0 %copy-start.33 = (bf16[1,4096,128]{2,1,0:T(8,128)(2,1)S(1)}, bf16[1,4096,128]{2,1,0:T(8,128)(2,1)}, u32[]{:S(2)}) copy-start(bf16[1,4096,128]{2,1,0:T(8,128)(2,1)} %param.35) | copy-start | bytes 3145732
  371.6 28.8 %collective-permute-start.14 = (bf16[1,1152,256]{1,2,0:T(8,128)(2,1)}, bf16[1,1152,256]{1,2,0:T(8,128)(2,1)S(1)}, u32[]{:S(2)}, u32[]{:S(2)}) collective-permute-start(bf16[1,1152,256]{1,2,0:T(8,128)(2,1)} %collective-permute-done.13), channel_id=1, source_target_pairs={{0,15},{1,0},{2,1},{3,2},{4,3},{5,4},{6,5},{7,6},{8,7},{9,8},{10,9... | collective-permute-start | bytes 1769480 | tf_op jit(solution)/shard_map/ppermute | solution.py:35
  413.9 31.9 %all-to-all-start.4 = ((bf16[16,2,1,36,128]{4,1,3,2,0:T(2,128)(2,1)}), bf16[16,2,1,36,128]{4,1,3,2,0:T(2,128)(2,1)S(1)}, u32[]{:S(2)}, u32[]{:S(2)}) async-start(bf16[16,2,1,36,128]{4,1,3,2,0:T(2,128)(2,1)} %copy.64), calls=%async_computation.4 | async-start | bytes 589824 | tf_op jit(solution)/shard_map/all_to_all | solution.py:137
  (21 other events, 348.1 us)
Sparse Core Ops, SparseCore 0:
  180.7 63.6 all-gather.9
